TPU v7x, 256 devices: a whole 4x4x8 slice. The times are simulated.
256 devices in a mesh: ep: 64 (over z, y, core), tp: 4 (over x).
Axes of the slice: x: 4, y: 4, z: 8, core: 2. Of those that a mesh axis runs over, the one named last changes fastest.
Arguments:
- query: bfloat16 [8192, 1536], P('ep', 'tp'), may hold values from -136 to 136
- latent: bfloat16 [8192, 512], P(('ep', 'tp')), may hold values from -6 to 6
- rope_key: bfloat16 [8192, 32], P(('ep', 'tp')), may hold values from -6 to 6
- latent_gain: float32 [512], replicated, may hold values from 0.1 to 1.9
- key_up: bfloat16 [512, 1024], P(None, 'tp'), may hold values from -0.25 to 0.25
- value_up: bfloat16 [512, 1024], P(None, 'tp'), may hold values from -2 to 2
- out_proj: bfloat16 [1024, 2048], replicated, may hold values from -0.1875 to 0.1875
- tokens: bfloat16 [16384, 2048], P(('ep', 'tp')), may hold values from -6 to 6
- moe_gain: float32 [2048], replicated, may hold values from 0.1 to 1.9
- routes: int32 [16384, 2], P(('ep', 'tp')), may hold values from 0 to 63, all different within a row; in each aligned block of 64 rows (0 to 63, 64 to 127, ...) at most 4 rows name the same one
- group_prob: float32 [16384], P(('ep', 'tp')), may hold values from 0.25 to 1
- expert_prob: float32 [16384, 2], P(('ep', 'tp')), may hold values from 0.02 to 1
- w_gate: bfloat16 [64, 2048, 1024], P('ep', None, 'tp'), may hold values from -0.125 to 0.125
- w_up: bfloat16 [64, 2048, 1024], P('ep', None, 'tp'), may hold values from -0.125 to 0.125
- w_down: bfloat16 [64, 1024, 2048], P('ep', 'tp'), may hold values from -0.1875 to 0.1875
Outputs:
- mixed: bfloat16 [8192, 2048], P(('ep', 'tp'))
- moe_out: bfloat16 [16384, 2048], P(('ep', 'tp'))
Inputs may be any that keep to these rules, and one draw needn't show every extreme that they name: `routes`: each row names 2 different experts; within the rows of one device no expert is named more than 4 times.
All inputs are finite; a program needn't handle non-finite values.
Results may differ from a plain program's by a relative error of at most 0.025.
Values may be sent and summed in bfloat16 or wider, within the bound.
No kernel may reach another device: no remote copies, remote signals or barrier semaphores. Data moves between devices by JAX's collectives and lax.ppermute only.
A program may use at most 128 MiB of HBM per device.

v0:
```python
import math
import jax
import jax.numpy as jnp
from jax import lax
from jax.sharding import PartitionSpec as P

NOPE = 64
ROPE_DIM = 32
V_DIM = 64
epsilon = 1e-06
rope_base = 10000.0
masked_value = -1e30


def in_one_piece(arrays, axis, dim, along):
    both = jnp.concatenate(arrays, axis=along)
    out, at, done = (lax.all_gather(both, axis, axis=dim, tiled=True), 0, [])
    for a in arrays:
        done.append(lax.slice_in_dim(out, at, at + a.shape[along], axis=along))
        at += a.shape[along]
    return tuple(done)


def split_up(value, dim, devices):
    before, after = (value.shape[:dim], value.shape[dim + 1 :])
    return jnp.moveaxis(value.reshape(*before, devices, -1, *after), dim, 0)


def sent_and_summed(value, axis, dim):
    devices = lax.axis_size(axis)
    parts = lax.all_to_all(split_up(value, dim, devices), axis, 0, 0, tiled=True)
    return jnp.sum(parts.astype(jnp.float32), axis=0)


def rms_scale(values, gain):
    widened = values.astype(jnp.float32)
    return widened * lax.rsqrt(jnp.mean(widened * widened, axis=-1, keepdims=True) + epsilon) * gain


def tables(positions, rope_width):
    half_width = rope_width // 2
    inverse = rope_base ** (-2.0 * jnp.arange(half_width, dtype=jnp.float32) / rope_width)
    angles = positions.astype(jnp.float32)[:, None] * inverse[None, :]
    return (jnp.cos(angles), jnp.sin(angles))


def rotate(values, cosine, sine):
    half_width = values.shape[-1] // 2
    lower = values[..., :half_width]
    upper = values[..., half_width:]
    return jnp.concatenate([lower * cosine - upper * sine, lower * sine + upper * cosine], axis=-1)


def keep_state(state_in):
    return state_in


def attend_block(running, query_rot, query_pos, key_part, value_part, rope_part):
    amount = key_part.shape[0]
    span_rows = math.gcd(amount, 1024)
    head_count = query_rot.shape[1]
    scale_factor = query_rot.shape[2] ** (-0.5)
    last_query = query_pos[-1]

    def update(state, block_at):
        row_begin = block_at * span_rows
        keys_here = lax.dynamic_slice_in_dim(key_part, row_begin, span_rows, 0).reshape(
            span_rows, head_count, -1
        )
        values_here = lax.dynamic_slice_in_dim(value_part, row_begin, span_rows, 0).reshape(
            span_rows, head_count, -1
        )
        rope_here = lax.dynamic_slice_in_dim(rope_part, row_begin, span_rows, 0)
        key_pos = row_begin + jnp.arange(span_rows, dtype=jnp.int32)

        def advance(state_in):
            top_old, totals, weighted = state_in
            shared = jnp.broadcast_to(
                rope_here[:, None, :], (span_rows, head_count, rope_here.shape[1])
            )
            full_keys = jnp.concatenate([keys_here, shared], axis=-1)
            scores = (
                jnp.einsum("qhd,khd->hqk", query_rot, full_keys, preferred_element_type=jnp.float32)
                * scale_factor
            )
            allowed = key_pos[None, :] <= query_pos[:, None]
            scores = jnp.where(allowed[None], scores, masked_value)
            top_new = jnp.maximum(top_old, jnp.max(scores, axis=-1))
            raised = jnp.where(allowed[None], jnp.exp(scores - top_new[..., None]), 0.0)
            factor = jnp.exp(top_old - top_new)
            totals = totals * factor + jnp.sum(raised, axis=-1)
            weighted = weighted * factor[..., None] + jnp.einsum(
                "hqk,khd->hqd",
                raised.astype(jnp.bfloat16),
                values_here,
                preferred_element_type=jnp.float32,
            )
            return (top_new, totals, weighted)

        return (lax.cond(key_pos[0] <= last_query, advance, keep_state, state), None)

    running, _ = lax.scan(update, running, jnp.arange(amount // span_rows))
    return running


def mixer_half(query, latent, rope_key, latent_gain, key_up, value_up, out_proj):
    query_rows = query.shape[0]
    own_rows = latent.shape[0]
    query_start = lax.axis_index("ep") * query_rows
    key_start = query_start + lax.axis_index("tp") * own_rows
    head_count = query.shape[1] // (NOPE + ROPE_DIM)
    normed = rms_scale(latent, latent_gain).astype(jnp.bfloat16)
    key_cos, key_sin = tables(key_start + jnp.arange(own_rows, dtype=jnp.int32), ROPE_DIM)
    rotated_key = rotate(rope_key.astype(jnp.float32), key_cos, key_sin).astype(jnp.bfloat16)
    query_pos = query_start + jnp.arange(query_rows, dtype=jnp.int32)
    query_cos, query_sin = tables(query_pos, ROPE_DIM)
    query_heads = query.reshape(query_rows, head_count, NOPE + ROPE_DIM)
    turned = rotate(
        query_heads[..., NOPE:].astype(jnp.float32), query_cos[:, None, :], query_sin[:, None, :]
    ).astype(jnp.bfloat16)
    query_rot = jnp.concatenate([query_heads[..., :NOPE], turned], axis=-1)
    last_query = query_start + query_rows - 1
    initial = (
        jnp.full((head_count, query_rows), masked_value, jnp.float32),
        jnp.zeros((head_count, query_rows), jnp.float32),
        jnp.zeros((head_count, query_rows, V_DIM), jnp.float32),
    )
    group_latent, group_rope = in_one_piece((normed, rotated_key), "tp", 0, 1)
    key_part = jnp.dot(group_latent, key_up, preferred_element_type=jnp.float32).astype(
        jnp.bfloat16
    )
    value_part = jnp.dot(group_latent, value_up, preferred_element_type=jnp.float32).astype(
        jnp.bfloat16
    )
    shard_rows = in_one_piece((key_part, value_part, group_rope), "ep", 0, 1)

    def compute(state_in):
        return attend_block(
            state_in, query_rot, query_pos, shard_rows[0], shard_rows[1], shard_rows[2]
        )

    running = lax.cond(jnp.int32(0) <= last_query, compute, keep_state, initial)
    totals = running[1]
    weighted = running[2]
    attention = (
        (weighted / totals[..., None])
        .transpose(1, 0, 2)
        .reshape(query_rows, head_count * V_DIM)
        .astype(jnp.bfloat16)
    )
    own_attention = lax.all_to_all(attention, "tp", split_axis=0, concat_axis=1, tiled=True)
    return jnp.dot(own_attention, out_proj, preferred_element_type=jnp.float32).astype(jnp.bfloat16)


def expert_half(tokens, moe_gain, routes, group_prob, expert_prob, w_gate, w_up, w_down):
    row_count, model_width = tokens.shape
    top_count = routes.shape[1]
    expert_count = lax.axis_size("ep")
    capacity = 2 * top_count * row_count // expert_count
    normed = rms_scale(tokens, moe_gain).astype(jnp.bfloat16)
    flat_routes = routes.reshape(-1)
    onehot = (flat_routes[:, None] == jnp.arange(expert_count, dtype=jnp.int32)[None, :]).astype(
        jnp.int32
    )
    earlier = jnp.cumsum(onehot, axis=0) - onehot
    slot_index = jnp.sum(earlier * onehot, axis=1)
    target = flat_routes * capacity + slot_index
    owner = target[None, :] == jnp.arange(expert_count * capacity, dtype=jnp.int32)[:, None]
    dispatch_table = jnp.any(
        owner.reshape(expert_count * capacity, row_count, top_count), axis=2
    ).astype(jnp.bfloat16)
    outgoing = jnp.dot(dispatch_table, normed, preferred_element_type=jnp.float32).astype(
        jnp.bfloat16
    )
    outgoing = outgoing.reshape(expert_count, capacity, model_width)
    arrived = lax.all_to_all(outgoing, "ep", split_axis=0, concat_axis=0, tiled=True)
    sources, slots, _ = arrived.shape
    flat_rows = arrived.reshape(sources * slots, model_width)
    shard_rows = lax.all_gather(flat_rows, "tp", axis=0, tiled=True)
    gate_values = jnp.dot(shard_rows, w_gate[0], preferred_element_type=jnp.float32)
    up_values = jnp.dot(shard_rows, w_up[0], preferred_element_type=jnp.float32)
    hidden = (jax.nn.silu(gate_values) * up_values).astype(jnp.bfloat16)

    def lower(offset, amount):
        return jnp.dot(hidden, w_down[0], preferred_element_type=jnp.float32)

    summed = sent_and_summed(
        lower(jnp.int32(0), sources * slots * lax.axis_size("tp")).astype(jnp.bfloat16), "tp", 0
    )
    result = summed.astype(jnp.bfloat16).reshape(sources, slots, model_width)
    returned = lax.all_to_all(result, "ep", split_axis=0, concat_axis=0, tiled=True)
    returned_flat = returned.reshape(expert_count * capacity, model_width)
    picked = returned_flat[target].reshape(row_count, top_count, model_width).astype(jnp.float32)
    shares = group_prob[:, None] * expert_prob / jnp.sum(expert_prob, axis=1, keepdims=True)
    return jnp.sum(shares[:, :, None] * picked, axis=1).astype(jnp.bfloat16)


def body(
    query,
    latent,
    rope_key,
    latent_gain,
    key_up,
    value_up,
    out_proj,
    tokens,
    moe_gain,
    routes,
    group_prob,
    expert_prob,
    w_gate,
    w_up,
    w_down,
):
    mixed = mixer_half(query, latent, rope_key, latent_gain, key_up, value_up, out_proj)
    moe_out = expert_half(tokens, moe_gain, routes, group_prob, expert_prob, w_gate, w_up, w_down)
    return (mixed, moe_out)


def solution(mesh):
    return jax.shard_map(
        body,
        mesh=mesh,
        in_specs=(
            P("ep", "tp"),
            P(("ep", "tp"), None),
            P(("ep", "tp"), None),
            P(),
            P(None, "tp"),
            P(None, "tp"),
            P(),
            P(("ep", "tp"), None),
            P(),
            P(("ep", "tp"), None),
            P(("ep", "tp")),
            P(("ep", "tp"), None),
            P("ep", None, "tp"),
            P("ep", None, "tp"),
            P("ep", "tp", None),
        ),
        out_specs=(P(("ep", "tp"), None), P(("ep", "tp"), None)),
        check_vma=False,
    )
```

profile of v0, /device:TPU:224, one launch (start us, length us, event | category | flops | bytes accessed | tf_op | source)
XLA Modules:
  0.0 333.0 jit_solution(12804921602035847933)
XLA Ops:
  10.1 1.5 convolution_convert_fusion.1
  12.0 36.0 %all_to_all.31 = bf16[64,4,2048]{2,1,0:T(4,128)(2,1)S(1)} all-to-all(bf16[64,4,2048]{2,1,0:T(4,128)(2,1)S(1)} %reshape.209), channel_id=1, replica_groups=mesh['ep'=64,'tp'=4] {'ep'}, dimensions={0} | all-to-all | bytes 2097152 | tf_op jit(solution)/shard_map/all_to_all | solution.py:176
  50.0 12.4 %all_gather.9 = bf16[128,544]{1,0:T(8,128)(2,1)S(1)} all-gather(bf16[32,544]{1,0:T(8,128)(2,1)S(1)} %pad_maximum_fusion.2), channel_id=1, replica_groups=mesh['ep'=64,'tp'=4] {'tp'}, dimensions={0}, use_global_device_ids=true | all-gather | bytes 174080 | tf_op jit(solution)/shard_map/all_gather | solution.py:17
  63.6 35.2 %all-gather.5.cloned.1.call-done = bf16[1024,2048]{1,0:T(8,128)(2,1)} async-done(((bf16[256,2048]{1,0:T(8,128)(2,1)}), bf16[1024,2048]{1,0:T(8,128)(2,1)}) %all-gather.5.cloned.1.call-update) | async-done | bytes 4194320 | tf_op jit(solution)/shard_map/all_gather | solution.py:179
  98.8 4.4 %fusion.20 = f32[1024,256]{1,0:T(8,128)} fusion(bf16[1024,2048]{1,0:T(8,128)(2,1)} %all-gather.5.cloned.1.call-done, bf16[1,2048,256]{2,1,0:T(8,128)(2,1)S(1)} %copy-done.9), kind=kOutput, calls=%fused_computation.36 | convolution fusion | flops 1073741824 | bytes 6291456 | tf_op jit(solution)/shard_map/dot_general | solution.py:180
  103.2 8.8 %convolution_convert_fusion = bf16[1024,2048]{1,0:T(8,128)(2,1)} fusion(bf16[1024,2048]{1,0:T(8,128)(2,1)} %all-gather.5.cloned.1.call-done, bf16[1,256,2048]{2,1,0:T(8,128)(2,1)S(1)} %copy-done, bf16[1,2048,256]{2,1,0:T(8,128)(2,1)S(1)} %copy-done.10, f32[1024,256]{1,0:T(8,128)} %fusion.20), kind=kOutput, calls=%fused_computation.27 | convolution fusion | flops 2151153664 | bytes 11534336 | tf_op jit(solution)/shard_map/dot_general | solution.py:185
  112.0 54.6 %all_to_all.32 = bf16[4,256,2048]{2,1,0:T(8,128)(2,1)} all-to-all(bf16[4,256,2048]{2,1,0:T(8,128)(2,1)} %bitcast.54), channel_id=1, replica_groups=mesh['ep'=64,'tp'=4] {'tp'}, dimensions={0} | all-to-all | bytes 8388608 | tf_op jit(solution)/shard_map/all_to_all | solution.py:31
  166.6 3.4 %reduce_sum.78 = bf16[256,2048]{1,0:T(8,128)(2,1)S(1)} reduce(bf16[4,256,2048]{2,1,0:T(8,128)(2,1)} %all_to_all.32, bf16[]{:T(256)} %constant.106.clone.1), dimensions={0}, to_apply=%region_14.15 | reduce | flops 1572864 | bytes 5242882 | tf_op jit(solution)/shard_map/reduce_sum | solution.py:32
  171.3 10.0 %all-to-all-start.3 = ((bf16[64,4,2048]{2,1,0:T(4,128)(2,1)}), bf16[64,4,2048]{2,1,0:T(4,128)(2,1)S(1)}, u32[]{:S(2)}, u32[]{:S(2)}) async-start(bf16[64,4,2048]{2,1,0:T(4,128)(2,1)} %reshape.212), calls=%async_computation.3 | async-start | bytes 2097152 | tf_op jit(solution)/shard_map/all_to_all | solution.py:191
  181.9 26.5 %all-to-all-done.3 = bf16[64,4,2048]{2,1,0:T(4,128)(2,1)S(1)} async-done(((bf16[64,4,2048]{2,1,0:T(4,128)(2,1)}), bf16[64,4,2048]{2,1,0:T(4,128)(2,1)S(1)}, u32[]{:S(2)}, u32[]{:S(2)}) %all-to-all-start.3) | async-done | bytes 1048608 | tf_op jit(solution)/shard_map/all_to_all | solution.py:191
  210.4 101.0 %conditional.2 = (f32[4,128]{1,0:T(4,128)}, f32[4,128,64]{1,2,0:T(8,128)}) conditional(s32[]{:T(128)} %convert_element_type.89, () %tuple.36, (bf16[8192,544]{1,0:T(8,128)(2,1)}, s32[]{:T(128)}, s32[128]{0:T(128)S(1)}, bf16[128,4,96]{0,2,1:T(8,128)(2,1)S(1)}) %tuple.37), branch_computations={%region_1.0_spmd, %region_2.9_spmd} | conditional | flops 176359552 | bytes 46872600 | solution.py:142
  210.4 12.9 %copy.45 = bf16[8192,544]{0,1:T(8,128)(2,1)} copy(bf16[8192,544]{1,0:T(8,128)(2,1)} %get-tuple-element.221) | data formatting | bytes 17825792 | tf_op jit(solution)/shard_map
  223.3 6.1 %fusion.53 = (bf16[8192,256]{0,1:T(8,128)(2,1)}, bf16[8192,256]{0,1:T(8,128)(2,1)}) fusion(bf16[8192,544]{0,1:T(8,128)(2,1)} %copy.45), kind=kLoop, calls=%fused_computation.97 | loop fusion | bytes 16777216 | tf_op jit(solution)/shard_map/slice | solution.py:19
  232.3 79.0 %while.13 = (s32[]{:T(128)}, f32[4,128]{1,0:T(4,128)S(1)}, f32[4,128]{1,0:T(4,128)}, f32[4,128,64]{1,2,0:T(8,128)}, s32[8]{0:T(128)S(1)}, /*index=5*/s32[]{:T(12...) while((s32[]{:T(128)}, f32[4,128]{1,0:T(4,128)S(1)}, ...), condition=%wide.region_8.8_spmd, body=%wide.region_3.7_spmd.sunk | while | flops 176359424 | bytes 11084641 | solution.py:102
  235.2 7.0 %conditional.4 = ((f32[4,128]{1,0:T(4,128)S(1)}, f32[4,128]{1,0:T(4,128)}, f32[4,128,64]{1,2,0:T(8,128)})) conditional(s32[]{:T(128)} %convert_element_type.152, (f32[4,128]{1,0:T(4,128)S(1)}, f32[4,128]{1,0:T(4,128)}, f32[4,128,64]{1,2,0:T(8,128)}) %tuple.61, (s32[1024]{0:T(1024)S(1)}, s32[128]{0:T(128)S(1)}, s32[]{:T(128)}, ...), branch_computations={%region_4.3_spmd, %region_5.6_spmd} | conditional | flops 176358400 | bytes 11080266 | solution.py:100
  235.2 1.9 constant_dynamic-slice_fusion
  238.6 1.3 multiply_add_fusion
  239.9 2.3 convolution_add_fusion
  245.1 7.0 %conditional.4 = ((f32[4,128]{1,0:T(4,128)S(1)}, f32[4,128]{1,0:T(4,128)}, f32[4,128,64]{1,2,0:T(8,128)})) conditional(s32[]{:T(128)} %convert_element_type.152, (f32[4,128]{1,0:T(4,128)S(1)}, f32[4,128]{1,0:T(4,128)}, f32[4,128,64]{1,2,0:T(8,128)}) %tuple.61, (s32[1024]{0:T(1024)S(1)}, s32[128]{0:T(128)S(1)}, s32[]{:T(128)}, ...), branch_computations={%region_4.3_spmd, %region_5.6_spmd} | conditional | flops 176358400 | bytes 11080266 | solution.py:100
  245.1 1.9 constant_dynamic-slice_fusion
  248.5 1.3 multiply_add_fusion
  249.8 2.3 convolution_add_fusion
  255.0 7.0 %conditional.4 = ((f32[4,128]{1,0:T(4,128)S(1)}, f32[4,128]{1,0:T(4,128)}, f32[4,128,64]{1,2,0:T(8,128)})) conditional(s32[]{:T(128)} %convert_element_type.152, (f32[4,128]{1,0:T(4,128)S(1)}, f32[4,128]{1,0:T(4,128)}, f32[4,128,64]{1,2,0:T(8,128)}) %tuple.61, (s32[1024]{0:T(1024)S(1)}, s32[128]{0:T(128)S(1)}, s32[]{:T(128)}, ...), branch_computations={%region_4.3_spmd, %region_5.6_spmd} | conditional | flops 176358400 | bytes 11080266 | solution.py:100
  255.0 1.9 constant_dynamic-slice_fusion
  258.4 1.3 multiply_add_fusion
  259.7 2.3 convolution_add_fusion
  264.9 7.0 %conditional.4 = ((f32[4,128]{1,0:T(4,128)S(1)}, f32[4,128]{1,0:T(4,128)}, f32[4,128,64]{1,2,0:T(8,128)})) conditional(s32[]{:T(128)} %convert_element_type.152, (f32[4,128]{1,0:T(4,128)S(1)}, f32[4,128]{1,0:T(4,128)}, f32[4,128,64]{1,2,0:T(8,128)}) %tuple.61, (s32[1024]{0:T(1024)S(1)}, s32[128]{0:T(128)S(1)}, s32[]{:T(128)}, ...), branch_computations={%region_4.3_spmd, %region_5.6_spmd} | conditional | flops 176358400 | bytes 11080266 | solution.py:100
  264.9 1.9 constant_dynamic-slice_fusion
  269.6 2.3 convolution_add_fusion
  274.8 7.0 %conditional.4 = ((f32[4,128]{1,0:T(4,128)S(1)}, f32[4,128]{1,0:T(4,128)}, f32[4,128,64]{1,2,0:T(8,128)})) conditional(s32[]{:T(128)} %convert_element_type.152, (f32[4,128]{1,0:T(4,128)S(1)}, f32[4,128]{1,0:T(4,128)}, f32[4,128,64]{1,2,0:T(8,128)}) %tuple.61, (s32[1024]{0:T(1024)S(1)}, s32[128]{0:T(128)S(1)}, s32[]{:T(128)}, ...), branch_computations={%region_4.3_spmd, %region_5.6_spmd} | conditional | flops 176358400 | bytes 11080266 | solution.py:100
  274.8 1.9 constant_dynamic-slice_fusion
  278.2 1.3 multiply_add_fusion
  279.4 2.3 convolution_add_fusion
  284.6 7.0 %conditional.4 = ((f32[4,128]{1,0:T(4,128)S(1)}, f32[4,128]{1,0:T(4,128)}, f32[4,128,64]{1,2,0:T(8,128)})) conditional(s32[]{:T(128)} %convert_element_type.152, (f32[4,128]{1,0:T(4,128)S(1)}, f32[4,128]{1,0:T(4,128)}, f32[4,128,64]{1,2,0:T(8,128)}) %tuple.61, (s32[1024]{0:T(1024)S(1)}, s32[128]{0:T(128)S(1)}, s32[]{:T(128)}, ...), branch_computations={%region_4.3_spmd, %region_5.6_spmd} | conditional | flops 176358400 | bytes 11080266 | solution.py:100
  284.7 1.9 constant_dynamic-slice_fusion
  288.1 1.3 multiply_add_fusion
  289.3 2.3 convolution_add_fusion
  294.5 7.0 %conditional.4 = ((f32[4,128]{1,0:T(4,128)S(1)}, f32[4,128]{1,0:T(4,128)}, f32[4,128,64]{1,2,0:T(8,128)})) conditional(s32[]{:T(128)} %convert_element_type.152, (f32[4,128]{1,0:T(4,128)S(1)}, f32[4,128]{1,0:T(4,128)}, f32[4,128,64]{1,2,0:T(8,128)}) %tuple.61, (s32[1024]{0:T(1024)S(1)}, s32[128]{0:T(128)S(1)}, s32[]{:T(128)}, ...), branch_computations={%region_4.3_spmd, %region_5.6_spmd} | conditional | flops 176358400 | bytes 11080266 | solution.py:100
  294.5 1.9 constant_dynamic-slice_fusion
  297.9 1.3 multiply_add_fusion
  299.2 2.3 convolution_add_fusion
  304.4 6.9 %conditional.4 = ((f32[4,128]{1,0:T(4,128)S(1)}, f32[4,128]{1,0:T(4,128)}, f32[4,128,64]{1,2,0:T(8,128)})) conditional(s32[]{:T(128)} %convert_element_type.152, (f32[4,128]{1,0:T(4,128)S(1)}, f32[4,128]{1,0:T(4,128)}, f32[4,128,64]{1,2,0:T(8,128)}) %tuple.61, (s32[1024]{0:T(1024)S(1)}, s32[128]{0:T(128)S(1)}, s32[]{:T(128)}, ...), branch_computations={%region_4.3_spmd, %region_5.6_spmd} | conditional | flops 176358400 | bytes 11080266 | solution.py:100
  304.4 1.8 constant_dynamic-slice_fusion
  309.1 2.3 convolution_add_fusion
  313.2 3.7 %all-to-all-start = ((bf16[4,32,256]{2,1,0:T(8,128)(2,1)}), bf16[4,32,256]{2,1,0:T(8,128)(2,1)S(1)}, u32[]{:S(2)}, u32[]{:S(2)}) async-start(bf16[4,32,256]{2,1,0:T(8,128)(2,1)} %convert_element_type.100), calls=%async_computation | async-start | bytes 131072 | tf_op jit(solution)/shard_map/all_to_all | solution.py:151
  316.9 2.2 multiply_reduce_fusion
  319.1 3.4 %all-to-all-done = bf16[4,32,256]{2,1,0:T(8,128)(2,1)S(1)} async-done(((bf16[4,32,256]{2,1,0:T(8,128)(2,1)}), bf16[4,32,256]{2,1,0:T(8,128)(2,1)S(1)}, u32[]{:S(2)}, u32[]{:S(2)}) %all-to-all-start) | async-done | bytes 65568 | tf_op jit(solution)/shard_map/all_to_all | solution.py:151
  322.5 3.7 %convolution_convert_fusion.2 = bf16[32,2048]{1,0:T(8,128)(2,1)} fusion(bf16[32,1024]{1,0:T(8,128)(2,1)S(1)} %bitcast.57, bf16[1024,2048]{1,0:T(8,128)(2,1)} %param.27), kind=kOutput, calls=%fused_computation.29 | convolution fusion | flops 134283264 | bytes 4390912 | tf_op jit(solution)/shard_map/dot_general | solution.py:152
  (166 shorter events, 37.9 us)
Async XLA Ops:
  7.2 96.0 %copy-start = (bf16[1,256,2048]{2,1,0:T(8,128)(2,1)S(1)}, bf16[1,256,2048]{2,1,0:T(8,128)(2,1)}, u32[]{:S(2)}) copy-start(bf16[1,256,2048]{2,1,0:T(8,128)(2,1)} %param.35) | copy-start | bytes 3145732
  7.2 91.6 %all-gather.5.cloned.1.call-start = ((), (), s32[]{:S(2)}) async-start(), calls=%async_computation.5 | async-start | bytes 5242880 | tf_op jit(solution)/shard_map/all_gather | solution.py:179
  48.0 1.3 copy-start.5
  48.0 1.7 copy-start.3
  48.0 1.8 copy-start.7
  48.1 14.4 %copy-start.1 = (bf16[512,256]{1,0:T(8,128)(2,1)S(1)}, bf16[512,256]{1,0:T(8,128)(2,1)}, u32[]{:S(2)}) copy-start(bf16[512,256]{1,0:T(8,128)(2,1)} %param.26) | copy-start | bytes 786436
  48.1 14.6 %copy-start.2 = (bf16[512,256]{1,0:T(8,128)(2,1)S(1)}, bf16[512,256]{1,0:T(8,128)(2,1)}, u32[]{:S(2)}) copy-start(bf16[512,256]{1,0:T(8,128)(2,1)} %param.25) | copy-start | bytes 786436
  49.2 49.6 %copy-start.9 = (bf16[1,2048,256]{2,1,0:T(8,128)(2,1)S(1)}, bf16[1,2048,256]{2,1,0:T(8,128)(2,1)}, u32[]{:S(2)}) copy-start(bf16[1,2048,256]{2,1,0:T(8,128)(2,1)} %param.33) | copy-start | bytes 3145732
  49.2 161.1 %all-gather.3.cloned.1.call-start = ((), (), s32[]{:S(2)}) async-start(), calls=%async_computation.4 | async-start | bytes 10649600 | tf_op jit(solution)/shard_map/all_gather | solution.py:17
  63.5 39.7 %copy-start.10 = (bf16[1,2048,256]{2,1,0:T(8,128)(2,1)S(1)}, bf16[1,2048,256]{2,1,0:T(8,128)(2,1)}, u32[]{:S(2)}) copy-start(bf16[1,2048,256]{2,1,0:T(8,128)(2,1)} %param.34) | copy-start | bytes 3145732
  170.0 11.3 %copy-start.4 = (bf16[128,384]{1,0:T(8,128)(2,1)S(1)}, bf16[128,384]{1,0:T(8,128)(2,1)}, u32[]{:S(2)}) copy-start(bf16[128,384]{1,0:T(8,128)(2,1)} %param.21) | copy-start | bytes 294916
  170.0 11.6 %copy-start.6 = (f32[64,2]{0,1:T(2,128)S(1)}, f32[64,2]{0,1:T(2,128)}, u32[]{:S(2)}) copy-start(f32[64,2]{0,1:T(2,128)} %param.32) | copy-start | bytes 1540
  170.0 11.6 %copy-start.8 = (f32[64]{0:T(128)S(1)}, f32[64]{0:T(128)}, u32[]{:S(2)}) copy-start(f32[64]{0:T(128)} %param.31) | copy-start | bytes 772
  171.3 37.2 %all-to-all-start.3 = ((bf16[64,4,2048]{2,1,0:T(4,128)(2,1)}), bf16[64,4,2048]{2,1,0:T(4,128)(2,1)S(1)}, u32[]{:S(2)}, u32[]{:S(2)}) async-start(bf16[64,4,2048]{2,1,0:T(4,128)(2,1)} %reshape.212), calls=%async_computation.3 | async-start | bytes 2097152 | tf_op jit(solution)/shard_map/all_to_all | solution.py:191
  313.2 9.3 %all-to-all-start = ((bf16[4,32,256]{2,1,0:T(8,128)(2,1)}), bf16[4,32,256]{2,1,0:T(8,128)(2,1)S(1)}, u32[]{:S(2)}, u32[]{:S(2)}) async-start(bf16[4,32,256]{2,1,0:T(8,128)(2,1)} %convert_element_type.100), calls=%async_computation | async-start | bytes 131072 | tf_op jit(solution)/shard_map/all_to_all | solution.py:151
Sparse Core Ops, SparseCore 0:
  49.4 49.3 all-gather.4
  102.1 91.5 all-gather.2
where the time goes:
time: 335 us; the launch traced here: 333 us
  blocking collectives  103 us (31%)
  waiting for transfers between devices  65.2 us (19%)
  local copies, waits for them, and re-layouts  54 us (16%)
  matrix products  42 us (13%)
  other arithmetic  25.7 us (8%)
  loops' own time  15 us (4%)
  between operations  14.4 us (4%)
  starting transfers between devices  13.8 us (4%)
    all_to_all x1, blocking collectives, sent_and_summed(): lax.all_to_all(split_up(value, dim, devices), axis, 0, 0, tiled=True)  54.6 us
    all_to_all x1, blocking collectives, expert_half(): lax.all_to_all(outgoing, 'ep', split_axis=0, concat_axis=0, tiled=True)  36 us
    all_gather x1, waiting for transfers between devices, expert_half(): shard_rows = lax.all_gather(flat_rows, 'tp', axis=0, tiled=True)  35.2 us
    all_to_all x1, waiting for transfers between devices, expert_half(): lax.all_to_all(result, 'ep', split_axis=0, concat_axis=0, tiled=True)  26.5 us
    dot_general x8, matrix products, advance(): jnp.einsum('hqk,khd->hqd', raised.astype(jnp.bfloat16), values_here, pref...  18.2 us
    dynamic_slice x8, local copies, waits for them, and re-layouts, update(): lax.dynamic_slice_in_dim(value_part, row_begin, span_rows, 0)  15 us
    another operation x1, loops' own time, attend_block(): running, _ = lax.scan(update, running, jnp.arange(amount // span_rows))  14.5 us
    another operation x3, local copies, waits for them, and re-layouts  13.1 us
  transfers between devices with their start and end apart: 4, of which 3 were waited for; matrix products, arithmetic and copies ran while one was open for 7% of the time, Pallas kernels for 0%

commit v1 on v0

--- a/solution.py
+++ b/solution.py
@@ -176,7 +176,10 @@
     arrived = lax.all_to_all(outgoing, "ep", split_axis=0, concat_axis=0, tiled=True)
     sources, slots, _ = arrived.shape
     flat_rows = arrived.reshape(sources * slots, model_width)
-    shard_rows = lax.all_gather(flat_rows, "tp", axis=0, tiled=True)
+    n_dev = lax.axis_size("tp")
+    blocks = jnp.stack([flat_rows for _ in range(n_dev)])
+    blocks = lax.all_to_all(blocks, "tp", split_axis=0, concat_axis=0)
+    shard_rows = jnp.concatenate(blocks, axis=0)
     gate_values = jnp.dot(shard_rows, w_gate[0], preferred_element_type=jnp.float32)
     up_values = jnp.dot(shard_rows, w_up[0], preferred_element_type=jnp.float32)
     hidden = (jax.nn.silu(gate_values) * up_values).astype(jnp.bfloat16)

time: 335 us -> 356 us (1.063)
  blocking collectives: 103 us -> 162 us
  waiting for transfers between devices: 65.2 us -> 29.7 us
  starting transfers between devices: 13.8 us -> 9.91 us
    all_to_all x0 -> x1, blocking collectives: none -> 52.8 us  [expert_half(): blocks = lax.all_to_all(blocks, 'tp', split_axis=0, concat_axis=0)]
    all_gather x1 -> x0, waiting for transfers between devices: 35.2 us -> none  [expert_half(): shard_rows = lax.all_gather(flat_rows, 'tp', axis=0, tiled=True)]
    all_to_all x1, blocking collectives: 36 us -> 42.4 us  [expert_half(): lax.all_to_all(outgoing, 'ep', split_axis=0, concat_axis=0, tiled=True)]
    another operation x3 -> x5, local copies, waits for them, and re-layouts: 13.1 us -> 14.9 us
  transfers between devices with their start and end apart: 4 -> 3, of which waited for: 3 -> 2; matrix products, arithmetic and copies ran while one was open for 7% -> 7% of each run, Pallas kernels for 0% -> 0%
where the time goes in v1:
time: 356 us; the launch traced here: 354 us
  blocking collectives  162 us (46%)
  local copies, waits for them, and re-layouts  57.5 us (16%)
  matrix products  39.4 us (11%)
  waiting for transfers between devices  29.7 us (8%)
  other arithmetic  25.9 us (7%)
  loops' own time  15.4 us (4%)
  between operations  14.4 us (4%)
  starting transfers between devices  9.91 us (3%)
    all_to_all x1, blocking collectives, sent_and_summed(): lax.all_to_all(split_up(value, dim, devices), axis, 0, 0, tiled=True)  54.1 us
    all_to_all x1, blocking collectives, expert_half(): blocks = lax.all_to_all(blocks, 'tp', split_axis=0, concat_axis=0)  52.8 us
    all_to_all x1, blocking collectives, expert_half(): lax.all_to_all(outgoing, 'ep', split_axis=0, concat_axis=0, tiled=True)  42.4 us
    all_to_all x1, waiting for transfers between devices, expert_half(): lax.all_to_all(result, 'ep', split_axis=0, concat_axis=0, tiled=True)  26.3 us
    dot_general x8, matrix products, advance(): jnp.einsum('hqk,khd->hqd', raised.astype(jnp.bfloat16), values_here, pref...  18 us
    dynamic_slice x8, local copies, waits for them, and re-layouts, update(): lax.dynamic_slice_in_dim(value_part, row_begin, span_rows, 0)  14.9 us
    another operation x1, loops' own time, attend_block(): running, _ = lax.scan(update, running, jnp.arange(amount // span_rows))  14.9 us
    another operation x3, local copies, waits for them, and re-layouts  13.1 us
  transfers between devices with their start and end apart: 3, of which 2 were waited for; matrix products, arithmetic and copies ran while one was open for 7% of the time, Pallas kernels for 0%

profile of v1, /device:TPU:224, one launch (start us, length us, event | category | flops | bytes accessed | tf_op | source)
XLA Modules:
  0.0 353.9 jit_solution(7917138097720309819)
XLA Ops:
  10.3 12.4 %all_gather.6 = bf16[128,544]{1,0:T(8,128)(2,1)S(1)} all-gather(bf16[32,544]{1,0:T(8,128)(2,1)S(1)} %pad_maximum_fusion.2), channel_id=1, replica_groups=mesh['ep'=64,'tp'=4] {'tp'}, dimensions={0}, use_global_device_ids=true | all-gather | bytes 174080 | tf_op jit(solution)/shard_map/all_gather | solution.py:17
  28.5 42.4 %all_to_all.36 = bf16[64,4,2048]{2,1,0:T(4,128)(2,1)} all-to-all(bf16[64,4,2048]{2,1,0:T(4,128)(2,1)S(1)} %reshape.211), channel_id=1, replica_groups=mesh['ep'=64,'tp'=4] {'ep'}, dimensions={0} | all-to-all | bytes 2097152 | tf_op jit(solution)/shard_map/all_to_all | solution.py:176
  70.9 1.3 stack_reshape.2
  72.8 52.8 %all_to_all.37 = bf16[4,256,2048]{2,1,0:T(8,128)(2,1)S(1)} all-to-all(bf16[4,256,2048]{2,1,0:T(8,128)(2,1)S(1)} %stack.3), channel_id=1, replica_groups=mesh['ep'=64,'tp'=4] {'tp'}, dimensions={0} | all-to-all | bytes 8388608 | tf_op jit(solution)/shard_map/all_to_all | solution.py:181
  125.6 2.0 copy-done.2
  128.8 8.6 %convolution_convert_fusion = bf16[1024,2048]{1,0:T(8,128)(2,1)} fusion(bf16[1024,2048]{1,0:T(8,128)(2,1)} %bitcast.56, bf16[1,256,2048]{2,1,0:T(8,128)(2,1)S(1)} %copy-done, bf16[1,2048,256]{2,1,0:T(8,128)(2,1)S(1)} %copy-done.9, f32[1024,256]{1,0:T(8,128)S(1)} %fusion.20), kind=kOutput, calls=%fused_computation.27 | convolution fusion | flops 2151153664 | bytes 11534336 | tf_op jit(solution)/shard_map/dot_general | solution.py:188
  137.4 54.1 %all_to_all.38 = bf16[4,256,2048]{2,1,0:T(8,128)(2,1)} all-to-all(bf16[4,256,2048]{2,1,0:T(8,128)(2,1)} %bitcast.57), channel_id=1, replica_groups=mesh['ep'=64,'tp'=4] {'tp'}, dimensions={0} | all-to-all | bytes 8388608 | tf_op jit(solution)/shard_map/all_to_all | solution.py:31
  191.5 3.1 reduce_sum.78
  195.8 6.6 %all-to-all-start.4 = ((bf16[64,4,2048]{2,1,0:T(4,128)(2,1)}), bf16[64,4,2048]{2,1,0:T(4,128)(2,1)S(1)}, u32[]{:S(2)}, u32[]{:S(2)}) async-start(bf16[64,4,2048]{2,1,0:T(4,128)(2,1)} %reshape.214), calls=%async_computation.4 | async-start | bytes 2097152 | tf_op jit(solution)/shard_map/all_to_all | solution.py:194
  203.1 26.3 %all-to-all-done.4 = bf16[64,4,2048]{2,1,0:T(4,128)(2,1)S(1)} async-done(((bf16[64,4,2048]{2,1,0:T(4,128)(2,1)}), bf16[64,4,2048]{2,1,0:T(4,128)(2,1)S(1)}, u32[]{:S(2)}, u32[]{:S(2)}) %all-to-all-start.4) | async-done | bytes 1048608 | tf_op jit(solution)/shard_map/all_to_all | solution.py:194
  231.3 101.3 %conditional.2 = (f32[4,128]{1,0:T(4,128)}, f32[4,128,64]{1,2,0:T(8,128)}) conditional(s32[]{:T(128)} %convert_element_type.89, () %tuple.36, (bf16[8192,544]{1,0:T(8,128)(2,1)}, s32[]{:T(128)}, s32[128]{0:T(128)S(1)}, bf16[128,4,96]{0,2,1:T(8,128)(2,1)S(1)}) %tuple.37), branch_computations={%region_1.0_spmd, %region_2.9_spmd} | conditional | flops 176359552 | bytes 46872600 | solution.py:142
  231.3 12.9 %copy.45 = bf16[8192,544]{0,1:T(8,128)(2,1)} copy(bf16[8192,544]{1,0:T(8,128)(2,1)} %get-tuple-element.221) | data formatting | bytes 17825792 | tf_op jit(solution)/shard_map
  244.2 6.0 %fusion.53 = (bf16[8192,256]{0,1:T(8,128)(2,1)}, bf16[8192,256]{0,1:T(8,128)(2,1)}) fusion(bf16[8192,544]{0,1:T(8,128)(2,1)} %copy.45), kind=kLoop, calls=%fused_computation.97 | loop fusion | bytes 16777216 | tf_op jit(solution)/shard_map/slice | solution.py:19
  253.2 79.3 %while.13 = (s32[]{:T(128)}, f32[4,128]{1,0:T(4,128)S(1)}, f32[4,128]{1,0:T(4,128)}, f32[4,128,64]{1,2,0:T(8,128)}, s32[8]{0:T(128)S(1)}, /*index=5*/s32[]{:T(12...) while((s32[]{:T(128)}, f32[4,128]{1,0:T(4,128)S(1)}, ...), condition=%wide.region_8.8_spmd, body=%wide.region_3.7_spmd.sunk | while | flops 176359424 | bytes 11084641 | solution.py:102
  256.2 6.9 %conditional.4 = ((f32[4,128]{1,0:T(4,128)S(1)}, f32[4,128]{1,0:T(4,128)}, f32[4,128,64]{1,2,0:T(8,128)})) conditional(s32[]{:T(128)} %convert_element_type.152, (f32[4,128]{1,0:T(4,128)S(1)}, f32[4,128]{1,0:T(4,128)}, f32[4,128,64]{1,2,0:T(8,128)}) %tuple.61, (s32[1024]{0:T(1024)S(1)}, s32[128]{0:T(128)S(1)}, s32[]{:T(128)}, ...), branch_computations={%region_4.3_spmd, %region_5.6_spmd} | conditional | flops 176358400 | bytes 11080266 | solution.py:100
  256.2 1.9 constant_dynamic-slice_fusion
  259.6 1.3 multiply_add_fusion
  260.9 2.2 convolution_add_fusion
  266.1 6.9 %conditional.4 = ((f32[4,128]{1,0:T(4,128)S(1)}, f32[4,128]{1,0:T(4,128)}, f32[4,128,64]{1,2,0:T(8,128)})) conditional(s32[]{:T(128)} %convert_element_type.152, (f32[4,128]{1,0:T(4,128)S(1)}, f32[4,128]{1,0:T(4,128)}, f32[4,128,64]{1,2,0:T(8,128)}) %tuple.61, (s32[1024]{0:T(1024)S(1)}, s32[128]{0:T(128)S(1)}, s32[]{:T(128)}, ...), branch_computations={%region_4.3_spmd, %region_5.6_spmd} | conditional | flops 176358400 | bytes 11080266 | solution.py:100
  266.1 1.9 constant_dynamic-slice_fusion
  269.5 1.3 multiply_add_fusion
  270.8 2.2 convolution_add_fusion
  276.0 6.9 %conditional.4 = ((f32[4,128]{1,0:T(4,128)S(1)}, f32[4,128]{1,0:T(4,128)}, f32[4,128,64]{1,2,0:T(8,128)})) conditional(s32[]{:T(128)} %convert_element_type.152, (f32[4,128]{1,0:T(4,128)S(1)}, f32[4,128]{1,0:T(4,128)}, f32[4,128,64]{1,2,0:T(8,128)}) %tuple.61, (s32[1024]{0:T(1024)S(1)}, s32[128]{0:T(128)S(1)}, s32[]{:T(128)}, ...), branch_computations={%region_4.3_spmd, %region_5.6_spmd} | conditional | flops 176358400 | bytes 11080266 | solution.py:100
  276.1 1.9 constant_dynamic-slice_fusion
  279.5 1.3 multiply_add_fusion
  280.7 2.2 convolution_add_fusion
  286.0 6.9 %conditional.4 = ((f32[4,128]{1,0:T(4,128)S(1)}, f32[4,128]{1,0:T(4,128)}, f32[4,128,64]{1,2,0:T(8,128)})) conditional(s32[]{:T(128)} %convert_element_type.152, (f32[4,128]{1,0:T(4,128)S(1)}, f32[4,128]{1,0:T(4,128)}, f32[4,128,64]{1,2,0:T(8,128)}) %tuple.61, (s32[1024]{0:T(1024)S(1)}, s32[128]{0:T(128)S(1)}, s32[]{:T(128)}, ...), branch_computations={%region_4.3_spmd, %region_5.6_spmd} | conditional | flops 176358400 | bytes 11080266 | solution.py:100
  286.0 1.9 constant_dynamic-slice_fusion
  289.4 1.3 multiply_add_fusion
  290.6 2.2 convolution_add_fusion
  295.9 6.9 %conditional.4 = ((f32[4,128]{1,0:T(4,128)S(1)}, f32[4,128]{1,0:T(4,128)}, f32[4,128,64]{1,2,0:T(8,128)})) conditional(s32[]{:T(128)} %convert_element_type.152, (f32[4,128]{1,0:T(4,128)S(1)}, f32[4,128]{1,0:T(4,128)}, f32[4,128,64]{1,2,0:T(8,128)}) %tuple.61, (s32[1024]{0:T(1024)S(1)}, s32[128]{0:T(128)S(1)}, s32[]{:T(128)}, ...), branch_computations={%region_4.3_spmd, %region_5.6_spmd} | conditional | flops 176358400 | bytes 11080266 | solution.py:100
  295.9 1.9 constant_dynamic-slice_fusion
  299.3 1.3 multiply_add_fusion
  300.6 2.2 convolution_add_fusion
  305.8 6.9 %conditional.4 = ((f32[4,128]{1,0:T(4,128)S(1)}, f32[4,128]{1,0:T(4,128)}, f32[4,128,64]{1,2,0:T(8,128)})) conditional(s32[]{:T(128)} %convert_element_type.152, (f32[4,128]{1,0:T(4,128)S(1)}, f32[4,128]{1,0:T(4,128)}, f32[4,128,64]{1,2,0:T(8,128)}) %tuple.61, (s32[1024]{0:T(1024)S(1)}, s32[128]{0:T(128)S(1)}, s32[]{:T(128)}, ...), branch_computations={%region_4.3_spmd, %region_5.6_spmd} | conditional | flops 176358400 | bytes 11080266 | solution.py:100
  305.8 1.9 constant_dynamic-slice_fusion
  310.5 2.2 convolution_add_fusion
  315.7 6.9 %conditional.4 = ((f32[4,128]{1,0:T(4,128)S(1)}, f32[4,128]{1,0:T(4,128)}, f32[4,128,64]{1,2,0:T(8,128)})) conditional(s32[]{:T(128)} %convert_element_type.152, (f32[4,128]{1,0:T(4,128)S(1)}, f32[4,128]{1,0:T(4,128)}, f32[4,128,64]{1,2,0:T(8,128)}) %tuple.61, (s32[1024]{0:T(1024)S(1)}, s32[128]{0:T(128)S(1)}, s32[]{:T(128)}, ...), branch_computations={%region_4.3_spmd, %region_5.6_spmd} | conditional | flops 176358400 | bytes 11080266 | solution.py:100
  315.8 1.9 constant_dynamic-slice_fusion
  319.1 1.3 multiply_add_fusion
  320.4 2.2 convolution_add_fusion
  325.7 6.9 %conditional.4 = ((f32[4,128]{1,0:T(4,128)S(1)}, f32[4,128]{1,0:T(4,128)}, f32[4,128,64]{1,2,0:T(8,128)})) conditional(s32[]{:T(128)} %convert_element_type.152, (f32[4,128]{1,0:T(4,128)S(1)}, f32[4,128]{1,0:T(4,128)}, f32[4,128,64]{1,2,0:T(8,128)}) %tuple.61, (s32[1024]{0:T(1024)S(1)}, s32[128]{0:T(128)S(1)}, s32[]{:T(128)}, ...), branch_computations={%region_4.3_spmd, %region_5.6_spmd} | conditional | flops 176358400 | bytes 11080266 | solution.py:100
  325.7 1.8 constant_dynamic-slice_fusion
  330.3 2.2 convolution_add_fusion
  334.4 3.3 all-to-all-start
  337.7 2.2 multiply_reduce_fusion
  339.9 3.4 all-to-all-done
  343.3 3.8 %convolution_convert_fusion.2 = bf16[32,2048]{1,0:T(8,128)(2,1)} fusion(bf16[32,1024]{1,0:T(8,128)(2,1)S(1)} %bitcast.60, bf16[1024,2048]{1,0:T(8,128)(2,1)} %param.27), kind=kOutput, calls=%fused_computation.29 | convolution fusion | flops 134283264 | bytes 4390912 | tf_op jit(solution)/shard_map/dot_general | solution.py:152
  (163 shorter events, 42.5 us)
Async XLA Ops:
  7.2 121.6 %copy-start = (bf16[1,256,2048]{2,1,0:T(8,128)(2,1)S(1)}, bf16[1,256,2048]{2,1,0:T(8,128)(2,1)}, u32[]{:S(2)}) copy-start(bf16[1,256,2048]{2,1,0:T(8,128)(2,1)} %param.35) | copy-start | bytes 3145732
  7.2 20.2 %copy-start.3 = (bf16[64,2048]{1,0:T(8,128)(2,1)S(1)}, bf16[64,2048]{1,0:T(8,128)(2,1)}, u32[]{:S(2)}) copy-start(bf16[64,2048]{1,0:T(8,128)(2,1)} %param.28) | copy-start | bytes 786436
  7.2 20.4 %copy-start.5 = (f32[2048]{0:T(1024)S(1)}, f32[2048]{0:T(1024)}, u32[]{:S(2)}) copy-start(f32[2048]{0:T(1024)} %param.29) | copy-start | bytes 24580
  7.2 224.0 %all-gather.2.cloned.1.call-start = ((), (), s32[]{:S(2)}) async-start(), calls=%async_computation.5 | async-start | bytes 10649600 | tf_op jit(solution)/shard_map/all_gather | solution.py:17
  72.8 54.8 %copy-start.8 = (bf16[1,2048,256]{2,1,0:T(8,128)(2,1)S(1)}, bf16[1,2048,256]{2,1,0:T(8,128)(2,1)}, u32[]{:S(2)}) copy-start(bf16[1,2048,256]{2,1,0:T(8,128)(2,1)} %param.33) | copy-start | bytes 3145732
  125.6 2.0 copy-start.2
  127.5 1.3 copy-start.9
  194.6 7.8 %copy-start.4 = (bf16[128,384]{1,0:T(8,128)(2,1)S(1)}, bf16[128,384]{1,0:T(8,128)(2,1)}, u32[]{:S(2)}) copy-start(bf16[128,384]{1,0:T(8,128)(2,1)} %param.21) | copy-start | bytes 294916
  194.6 8.1 %copy-start.6 = (f32[64,2]{0,1:T(2,128)S(1)}, f32[64,2]{0,1:T(2,128)}, u32[]{:S(2)}) copy-start(f32[64,2]{0,1:T(2,128)} %param.32) | copy-start | bytes 1540
  194.6 8.1 %copy-start.7 = (f32[64]{0:T(128)S(1)}, f32[64]{0:T(128)}, u32[]{:S(2)}) copy-start(f32[64]{0:T(128)} %param.31) | copy-start | bytes 772
  195.8 33.5 %all-to-all-start.4 = ((bf16[64,4,2048]{2,1,0:T(4,128)(2,1)}), bf16[64,4,2048]{2,1,0:T(4,128)(2,1)S(1)}, u32[]{:S(2)}, u32[]{:S(2)}) async-start(bf16[64,4,2048]{2,1,0:T(4,128)(2,1)} %reshape.214), calls=%async_computation.4 | async-start | bytes 2097152 | tf_op jit(solution)/shard_map/all_to_all | solution.py:194
  334.4 8.9 %all-to-all-start = ((bf16[4,32,256]{2,1,0:T(8,128)(2,1)}), bf16[4,32,256]{2,1,0:T(8,128)(2,1)S(1)}, u32[]{:S(2)}, u32[]{:S(2)}) async-start(bf16[4,32,256]{2,1,0:T(8,128)(2,1)} %convert_element_type.100), calls=%async_computation | async-start | bytes 131072 | tf_op jit(solution)/shard_map/all_to_all | solution.py:151
  343.3 3.8 %copy-start.1 = (bf16[1,256,2048]{2,1,0:T(8,128)(2,1)S(1)}, bf16[1,256,2048]{2,1,0:T(8,128)(2,1)}, u32[]{:S(2)}) copy-start(bf16[1,256,2048]{2,1,0:T(8,128)(2,1)} %param.35) | copy-start | bytes 3145732
Sparse Core Ops, SparseCore 0:
  25.8 88.9 all-gather.1
